TPU v7x, 32 devices: a whole 2x2x4 slice. The times are simulated.
32 devices in a mesh: sp: 16 (over z, y, x), tp: 2 (over core).
Axes of the slice: x: 2, y: 2, z: 4, core: 2. Of those that a mesh axis runs over, the one named last changes fastest.
Arguments:
- residual: bfloat16 [2048, 2048], P(('sp', 'tp')), may hold values from -6 to 6
- query_wide: bfloat16 [2048, 1024], P('sp', 'tp'), may hold values from -6 to 6
- key_wide: bfloat16 [2048, 1024], P('sp', 'tp'), may hold values from -6 to 6
- value_wide: bfloat16 [2048, 2048], P('sp', 'tp'), may hold values from -6 to 6
- outgate_wide: bfloat16 [2048, 2048], P('sp', 'tp'), may hold values from -6 to 6
- gating_wide: float32 [3, 8, 2048], P(None, 'tp', 'sp'), may hold values from -4 to 240, as said below
- gain_wide: bfloat16 [2048], P('tp'), may hold values from 0.099609375 to 1.8984375
- readout_wide: bfloat16 [2048, 2048], P('tp'), may hold values from -0.109375 to 0.109375
- query_narrow: bfloat16 [2048, 512], P('sp', 'tp'), may hold values from -6 to 6
- key_narrow: bfloat16 [2048, 512], P('sp', 'tp'), may hold values from -6 to 6
- value_narrow: bfloat16 [2048, 1024], P('sp', 'tp'), may hold values from -6 to 6
- outgate_narrow: bfloat16 [2048, 1024], P('sp', 'tp'), may hold values from -6 to 6
- gating_narrow: float32 [3, 8, 2048], P(None, 'tp', 'sp'), may hold values from -4 to 240, as said below
- gain_narrow: bfloat16 [1024], P('tp'), may hold values from 0.099609375 to 1.8984375
- readout_narrow: bfloat16 [1024, 2048], P('tp'), may hold values from -0.109375 to 0.109375
- norm_gain: bfloat16 [2048], replicated, may hold values from 0.099609375 to 1.8984375
- gate_weight: bfloat16 [2048, 5632], P('sp', 'tp'), may hold values from -0.125 to 0.125
- up_weight: bfloat16 [2048, 5632], P('sp', 'tp'), may hold values from -0.125 to 0.125
- down_weight: bfloat16 [5632, 2048], P('tp', 'sp'), may hold values from -0.078125 to 0.078125
Outputs:
- mixed_out: bfloat16 [2048, 2048], P(('sp', 'tp'))
Inputs may be any that keep to these rules, and one draw needn't show every extreme that they name: `gating_wide`: row 0 holds input gate pre-activations, row 1 forget gate pre-activations, row 2 an added log-decay that is zero or negative. `gating_narrow`: row 0 holds input gate pre-activations, row 1 forget gate pre-activations, row 2 an added log-decay that is zero or negative.
All inputs are finite; a program needn't handle non-finite values.
Results may differ from a plain program's by a relative error of at most 0.017.
Values may be sent and summed in bfloat16 or wider, within the bound.
No kernel may reach another device: no remote copies, remote signals or barrier semaphores. Data moves between devices by JAX's collectives and lax.ppermute only.
A program may use at most 128 MiB of HBM per device.

v0:
```python
import jax
import jax.numpy as jnp
from jax import lax
from jax.sharding import PartitionSpec as P

DK_A = 128
DK_B = 64
BLOCK = 64


def entering(value, axis, combine, identity):
    length, here = (lax.axis_size(axis), lax.axis_index(axis))
    everything = jax.tree.map(lambda part: lax.all_gather(part, axis), value)
    start = jax.tree.map(
        lambda part, zero: jnp.broadcast_to(jnp.asarray(zero, part.dtype), part.shape),
        value,
        identity,
    )

    def step(k, before):
        reached = k < here
        new = combine(before, jax.tree.map(lambda part: part[k], everything))
        return jax.tree.map(lambda a, b: jnp.where(reached, a, b), new, before)

    return lax.fori_loop(0, length, step, start)


def local_pass(query, key_rows, value, gating, key_size):
    rows = query.shape[0]
    attention_tally = gating.shape[1]
    value_size = value.shape[1] // attention_tally
    nblocks = rows // BLOCK
    scale = key_size ** (-0.5)
    queries = query.reshape(nblocks, BLOCK, attention_tally, key_size)
    keys_all = key_rows.reshape(nblocks, BLOCK, attention_tally, key_size)
    values_all = value.reshape(nblocks, BLOCK, attention_tally, value_size)
    incoming_matrix = jnp.moveaxis(gating[0].reshape(attention_tally, nblocks, BLOCK), 1, 0)
    forget_log = jax.nn.log_sigmoid(gating[1]) + gating[2]
    forgets = jnp.moveaxis(forget_log.reshape(attention_tally, nblocks, BLOCK), 1, 0)
    causal = jnp.tril(jnp.ones((BLOCK, BLOCK), dtype=bool))

    def advance(carry, blocks):
        memory, level = carry
        q_block, k_block, v_block, in_block, f_block = blocks
        cumul = jnp.cumsum(f_block, axis=-1)
        logits = cumul[:, :, None] - cumul[:, None, :] + in_block[:, None, :]
        logits = jnp.where(causal, logits, -jnp.inf)
        carried = cumul + level[:, None]
        stab = jnp.maximum(carried, jnp.max(logits, axis=-1))
        weights = jnp.exp(logits - stab[:, :, None])
        scores = (
            jnp.einsum("thd,shd->hts", q_block, k_block, preferred_element_type=jnp.float32) * scale
        )
        weighted = (scores * weights).astype(jnp.bfloat16)
        within = jnp.einsum("hts,shv->thv", weighted, v_block, preferred_element_type=jnp.float32)
        earlier = jnp.einsum(
            "thd,hdv->thv", q_block.astype(jnp.float32), memory, precision=lax.Precision.HIGHEST
        )
        earlier = earlier * jnp.exp(carried - stab).T[:, :, None]
        last = cumul[:, -1]
        tail = last[:, None] - cumul + in_block
        level_new = jnp.maximum(last + level, jnp.max(tail, axis=-1))
        tail_weights = jnp.exp(tail - level_new[:, None]) * scale
        scaled_keys = (k_block * tail_weights.T[:, :, None]).astype(jnp.bfloat16)
        memory_new = jnp.exp(last + level - level_new)[:, None, None] * memory
        memory_new = memory_new + jnp.einsum(
            "shd,shv->hdv", scaled_keys, v_block, preferred_element_type=jnp.float32
        )
        return ((memory_new, level_new), (within + earlier, stab))

    init = (
        jnp.zeros((attention_tally, key_size, value_size), jnp.float32),
        jnp.full((attention_tally,), -1e30, jnp.float32),
    )
    (memory_end, level_end), (raw, stabs) = lax.scan(
        advance, init, (queries, keys_all, values_all, incoming_matrix, forgets)
    )
    raw = raw.reshape(rows, attention_tally, value_size)
    stabs = jnp.moveaxis(stabs, 0, 1).reshape(attention_tally, rows)
    running = jnp.cumsum(forget_log, axis=1)
    return (raw, stabs, running, memory_end, level_end, running[:, -1])


def merge_states(earlier, later):
    merged = []
    for group in range(2):
        memory_e, level_e, total_e = earlier[3 * group : 3 * group + 3]
        memory_l, level_l, total_l = later[3 * group : 3 * group + 3]
        level = jnp.maximum(level_e + total_l, level_l)
        memory = (
            jnp.exp(level_e + total_l - level)[:, None, None] * memory_e
            + jnp.exp(level_l - level)[:, None, None] * memory_l
        )
        merged.extend([memory, level, total_e + total_l])
    return tuple(merged)


def finish_group(query, raw, stabs, running, memory_in, level_in, gain, outgate, key_size):
    rows, attention_tally, value_size = raw.shape
    shifted = running + level_in[:, None]
    stab = jnp.maximum(stabs, shifted)
    own = raw * jnp.exp(stabs - stab).T[:, :, None]
    queries = query.reshape(rows, attention_tally, key_size).astype(jnp.float32)
    incoming = jnp.einsum("thd,hdv->thv", queries, memory_in, precision=lax.Precision.HIGHEST)
    total = own + incoming * jnp.exp(shifted - stab).T[:, :, None]
    normal_raw = total * lax.rsqrt(jnp.mean(total * total, axis=-1, keepdims=True) + 1e-06)
    flat = normal_raw.reshape(rows, attention_tally * value_size)
    flat = flat * gain.astype(jnp.float32) * jax.nn.sigmoid(outgate.astype(jnp.float32))
    return flat.astype(jnp.bfloat16)


def norm_rows(middle_f, norm_gain):
    normed = middle_f * lax.rsqrt(jnp.mean(middle_f * middle_f, axis=-1, keepdims=True) + 1e-06)
    return (normed * norm_gain.astype(jnp.float32)).astype(jnp.bfloat16)


def body(
    residual,
    query_wide,
    key_wide,
    value_wide,
    outgate_wide,
    gating_wide,
    gain_wide,
    readout_wide,
    query_narrow,
    key_narrow,
    value_narrow,
    outgate_narrow,
    gating_narrow,
    gain_narrow,
    readout_narrow,
    norm_gain,
    gate_weight,
    up_weight,
    down_weight,
):
    raw_w, stabs_w, running_w, memory_w, level_w, total_w = local_pass(
        query_wide, key_wide, value_wide, gating_wide, DK_A
    )
    raw_n, stabs_n, running_n, memory_n, level_n, total_n = local_pass(
        query_narrow, key_narrow, value_narrow, gating_narrow, DK_B
    )
    carried = entering(
        (memory_w, level_w, total_w, memory_n, level_n, total_n),
        "sp",
        merge_states,
        (
            jnp.zeros_like(memory_w),
            jnp.full_like(level_w, -1e30),
            jnp.zeros_like(total_w),
            jnp.zeros_like(memory_n),
            jnp.full_like(level_n, -1e30),
            jnp.zeros_like(total_n),
        ),
    )
    gated_w = finish_group(
        query_wide, raw_w, stabs_w, running_w, carried[0], carried[1], gain_wide, outgate_wide, DK_A
    )
    gated_n = finish_group(
        query_narrow,
        raw_n,
        stabs_n,
        running_n,
        carried[3],
        carried[4],
        gain_narrow,
        outgate_narrow,
        DK_B,
    )
    mixed = lax.psum_scatter(
        (
            jnp.dot(gated_w, readout_wide, preferred_element_type=jnp.float32)
            + jnp.dot(gated_n, readout_narrow, preferred_element_type=jnp.float32)
        ).astype(jnp.bfloat16),
        "tp",
        scatter_dimension=0,
        tiled=True,
    ).astype(jnp.float32)
    middle_f = (residual.astype(jnp.float32) + mixed).astype(jnp.bfloat16).astype(jnp.float32)
    normed = norm_rows(middle_f, norm_gain)
    all_rows = lax.all_gather(normed, "tp", axis=0, tiled=True)
    gate = jnp.dot(
        all_rows,
        lax.all_gather(gate_weight, "sp", axis=0, tiled=True),
        preferred_element_type=jnp.float32,
    )
    upper = jnp.dot(
        all_rows,
        lax.all_gather(up_weight, "sp", axis=0, tiled=True),
        preferred_element_type=jnp.float32,
    )
    hidden = (jax.nn.silu(gate) * upper).astype(jnp.bfloat16)
    terms = jnp.dot(
        hidden,
        lax.all_gather(down_weight, "sp", axis=1, tiled=True),
        preferred_element_type=jnp.float32,
    )
    back = lax.psum_scatter(
        terms.astype(jnp.bfloat16), "tp", scatter_dimension=0, tiled=True
    ).astype(jnp.float32)
    return (middle_f + back).astype(jnp.bfloat16)


def solution(mesh):
    in_specs = (
        P(("sp", "tp"), None),
        P("sp", "tp"),
        P("sp", "tp"),
        P("sp", "tp"),
        P("sp", "tp"),
        P(None, "tp", "sp"),
        P("tp"),
        P("tp", None),
        P("sp", "tp"),
        P("sp", "tp"),
        P("sp", "tp"),
        P("sp", "tp"),
        P(None, "tp", "sp"),
        P("tp"),
        P("tp", None),
        P(),
        P("sp", "tp"),
        P("sp", "tp"),
        P("tp", "sp"),
    )
    out_specs = P(("sp", "tp"), None)
    return jax.shard_map(body, mesh=mesh, in_specs=in_specs, out_specs=out_specs, check_vma=False)
```

profile of v0, /device:TPU:0, one launch (start us, length us, event | category | flops | bytes accessed | tf_op | source)
XLA Modules:
  0.0 764.9 jit_solution(13011065428079746588)
XLA Ops:
  10.6 5.3 while.55
  19.7 19.3 %while.54 = (s32[]{:T(128)}, f32[4,128,256]{2,1,0:T(8,128)S(1)}, f32[4]{0:T(128)}, f32[2,64,4,256]{3,1,0,2:T(8,128)}, f32[2,4,64]{2,1,0:T(4,128)}, /*index=5*/f3...) while((s32[]{:T(128)}, f32[4,128,256]{2,1,0:T(8,128)S(1)}, ...), condition=%wide.region_4.5_spmd.clone, body=%wide.region_0.4_spmd.clone.sunk | while | flops 130980880 | bytes 3455009 | solution.py:75
  21.8 1.3 add_maximum_fusion.4
  25.7 1.0 fusion.152
  27.8 1.3 fusion.153
  31.8 1.3 add_maximum_fusion.4
  37.8 1.2 fusion.153
  40.0 1.6 copy.70
  41.5 1.3 dynamic-slice
  48.0 44.1 %all-reduce.4 = (f32[64]{0:T(128)S(1)}, f32[64]{0:T(128)S(1)}, f32[64]{0:T(128)S(1)}, f32[64]{0:T(128)S(1)}) all-reduce(f32[64]{0:T(128)S(1)} %dynamic-update-slice, f32[64]{0:T(128)S(1)} %dynamic-update-slice.1, f32[64]{0:T(128)S(1)} %dynamic-update-slice.2, f32[64]{0:T(128)S(1)} %dynamic-update-slice.3), channel_id=2, replica_groups=mesh['sp'=16,'tp'=2] {'sp'}, use_global_device_ids=true, to_apply=%add | all-reduce | flops 256 | bytes 2048
  96.3 1.1 copy.69
  97.4 1.2 copy.63
  98.7 1.3 convert_element_type.74
  99.9 1.3 convert_element_type.77
  101.2 93.0 %all-gather.18.cloned.1.call-done = f32[64,128,256]{2,1,0:T(8,128)} async-done(((f32[4,128,256]{2,1,0:T(8,128)}), f32[64,128,256]{2,1,0:T(8,128)}) %all-gather.18.cloned.1.call-update) | async-done | bytes 8388624 | tf_op jit(solution)/shard_map/all_gather | solution.py:13
  194.2 56.7 %while.56 = (s32[]{:T(128)}, f32[4,128,256]{2,1,0:T(8,128)S(1)}, f32[4]{0:T(128)}, f32[4,64,128]{2,1,0:T(8,128)S(1)}, f32[4]{0:T(128)}, /*index=5*/s32[]{:T(128)...) while((s32[]{:T(128)}, f32[4,128,256]{2,1,0:T(8,128)S(1)}, ...), condition=%wide.region_13.14_spmd.clone, body=%wide.region_12.13_spmd.clone.sunk | while | flops 819260 | bytes 1966609 | solution.py:25
  194.2 1.3 broadcast_select_fusion.9
  195.5 1.2 fusion.162
  197.8 1.3 broadcast_select_fusion.9
  199.1 1.2 fusion.162
  201.3 1.3 broadcast_select_fusion.9
  202.6 1.2 fusion.162
  204.9 1.3 broadcast_select_fusion.9
  206.2 1.2 fusion.162
  208.4 1.3 broadcast_select_fusion.9
  209.7 1.2 fusion.162
  212.0 1.3 broadcast_select_fusion.9
  213.3 1.2 fusion.162
  215.5 1.3 broadcast_select_fusion.9
  216.8 1.2 fusion.162
  219.1 1.3 broadcast_select_fusion.9
  220.4 1.2 fusion.162
  222.6 1.3 broadcast_select_fusion.9
  223.9 1.2 fusion.162
  226.2 1.3 broadcast_select_fusion.9
  227.5 1.2 fusion.162
  229.7 1.3 broadcast_select_fusion.9
  231.0 1.2 fusion.162
  233.2 1.3 broadcast_select_fusion.9
  234.5 1.2 fusion.162
  236.8 1.3 broadcast_select_fusion.9
  238.1 1.2 fusion.162
  240.3 1.3 broadcast_select_fusion.9
  241.6 1.2 fusion.162
  243.9 1.3 broadcast_select_fusion.9
  245.2 1.2 fusion.162
  247.4 1.3 broadcast_select_fusion.9
  248.7 1.2 fusion.162
  251.8 1.3 multiply_reduce_fusion.1
  253.7 1.1 copy.71
  254.8 1.5 multiply_reduce_fusion
  256.7 3.0 fusion.76
  259.8 1.3 fusion.67
  262.9 4.4 reduce-scatter.3.cloned.1.call-done
  267.4 1.1 fusion.72
  268.5 1.1 fusion.74
  269.6 2.4 all_gather.52
  272.0 140.6 %all-gather.12.cloned.1.call-done = bf16[2048,2816]{1,0:T(8,128)(2,1)} async-done(((bf16[128,2816]{1,0:T(8,128)(2,1)}), bf16[2048,2816]{1,0:T(8,128)(2,1)}) %all-gather.12.cloned.1.call-update) | async-done | bytes 11534352 | tf_op jit(solution)/shard_map/all_gather | solution.py:185
  412.5 7.1 fusion.118
  419.6 135.2 %all-gather.14.cloned.1.call-done = bf16[2048,2816]{1,0:T(8,128)(2,1)} async-done(((bf16[128,2816]{1,0:T(8,128)(2,1)}), bf16[2048,2816]{1,0:T(8,128)(2,1)}) %all-gather.14.cloned.1.call-update) | async-done | bytes 11534352 | tf_op jit(solution)/shard_map/all_gather | solution.py:190
  554.8 182.8 %all-gather.16.cloned.1.call-done = bf16[2816,2048]{1,0:T(8,128)(2,1)} async-done(((bf16[2816,128]{1,0:T(8,128)(2,1)}), bf16[2816,2048]{1,0:T(8,128)(2,1)}) %all-gather.16.cloned.1.call-update) | async-done | bytes 11534352 | tf_op jit(solution)/shard_map/all_gather | solution.py:196
  737.6 12.4 %convolution_convert_fusion = bf16[128,2048]{1,0:T(8,128)(2,1)} fusion(bf16[2816,2048]{1,0:T(8,128)(2,1)} %all-gather.16.cloned.1.call-done, bf16[128,2048]{1,0:T(8,128)(2,1)S(1)} %all_gather.52, bf16[2048,2816]{1,0:T(8,128)(2,1)} %all-gather.14.cloned.1.call-done, f32[128,2816]{1,0:T(8,128)} %fusion.118), kind=kOutput, calls=%fused_computation.130 | convolution fusion | flops 2955214848 | bytes 25559040 | tf_op jit(solution)/shard_map/dot_general | solution.py:194
  750.0 6.3 reduce-scatter.5.cloned.1.call-done
  756.3 1.7 fusion.75
  (224 shorter events, 55.6 us)
Async XLA Ops:
  6.5 253.2 %copy-start = (bf16[512,2048]{1,0:T(8,128)(2,1)S(1)}, bf16[512,2048]{1,0:T(8,128)(2,1)}, u32[]{:S(2)}) copy-start(bf16[512,2048]{1,0:T(8,128)(2,1)} %param.39) | copy-start | bytes 6291460
  6.5 94.7 %all-gather.20.cloned.1.call-start = ((), (), s32[]{:S(2)}) async-start(), calls=%async_computation.8 | async-start | bytes 2228224 | tf_op jit(solution)/shard_map/all_gather | solution.py:13
  10.6 6.1 copy-start.15
  10.6 7.0 copy-start.8
  10.6 7.1 copy-start.11
  10.6 7.2 copy-start.7
  15.9 0.6 copy-start.3
  15.9 1.6 copy-start.12
  15.9 1.6 copy-start.16
  16.6 177.6 %all-gather.18.cloned.1.call-start = ((), (), s32[]{:S(2)}) async-start(), calls=%async_computation.7 | async-start | bytes 8912896 | tf_op jit(solution)/shard_map/all_gather | solution.py:13
  20.4 2.7 copy-start.6
  21.0 2.1 copy-start.9
  29.8 3.3 copy-start.6
  31.0 2.1 copy-start.9
  39.0 0.8 copy-start.2
  39.9 227.5 %reduce-scatter.3.cloned.1.call-start = ((), (), s32[]{:S(2)}) async-start(), calls=%async_computation.2 | async-start | bytes 786432 | tf_op jit(solution)/shard_map/reduce_scatter | solution.py:171
  46.1 51.3 %copy-start.13 = (f32[4,128]{1,0:T(4,128)}, f32[4,128]{1,0:T(4,128)S(1)}, u32[]{:S(2)}) copy-start(f32[4,128]{1,0:T(4,128)S(1)} %reduce_window_sum.38) | copy-start | bytes 6148
  47.5 49.9 %copy-start.14 = (f32[4,128]{1,0:T(4,128)}, f32[4,128]{1,0:T(4,128)S(1)}, u32[]{:S(2)}) copy-start(f32[4,128]{1,0:T(4,128)S(1)} %reduce_window_sum.39) | copy-start | bytes 6148
  251.0 5.7 copy-start.19
  256.4 3.3 copy-start.10
  256.4 3.3 copy-start.17
  259.7 3.2 copy-start.18
  259.7 7.6 copy-start.4
  261.1 151.4 %all-gather.12.cloned.1.call-start = ((), (), s32[]{:S(2)}) async-start(), calls=%async_computation.3 | async-start | bytes 12255232 | tf_op jit(solution)/shard_map/all_gather | solution.py:185
  261.7 293.1 %all-gather.14.cloned.1.call-start = ((), (), s32[]{:S(2)}) async-start(), calls=%async_computation.4 | async-start | bytes 12255232 | tf_op jit(solution)/shard_map/all_gather | solution.py:190
  262.3 475.3 %all-gather.16.cloned.1.call-start = ((), (), s32[]{:S(2)}) async-start(), calls=%async_computation.5 | async-start | bytes 12255232 | tf_op jit(solution)/shard_map/all_gather | solution.py:196
  262.8 493.5 %reduce-scatter.5.cloned.1.call-start = ((), (), s32[]{:S(2)}) async-start(), calls=%async_computation.6 | async-start | bytes 786432 | tf_op jit(solution)/shard_map/reduce_scatter | solution.py:199
  419.6 336.7 %copy-start.5 = (bf16[64,2048]{1,0:T(8,128)(2,1)S(1)}, bf16[64,2048]{1,0:T(8,128)(2,1)}, u32[]{:S(2)}) copy-start(bf16[64,2048]{1,0:T(8,128)(2,1)} %reduce-scatter.3.cloned.1.call-done) | copy-start | bytes 786436
  737.6 20.5 %copy-start.1 = (bf16[512,2048]{1,0:T(8,128)(2,1)S(1)}, bf16[512,2048]{1,0:T(8,128)(2,1)}, u32[]{:S(2)}) copy-start(bf16[512,2048]{1,0:T(8,128)(2,1)} %param.39) | copy-start | bytes 6291460
Sparse Core Ops, SparseCore 0:
  16.7 63.6 all-gather.19
  83.2 111.0 all-gather.17
  261.2 6.0 reduce-scatter.2
  270.0 142.5 all-gather.11
  415.1 139.5 all-gather.13
  557.3 180.2 all-gather.15
  750.2 6.0 reduce-scatter.4
where the time goes:
time: 768 us; the launch traced here: 765 us
  waiting for transfers between devices  564 us (73%)
  other arithmetic  79.1 us (10%)
  blocking collectives  46.5 us (6%)
  matrix products  35.6 us (5%)
  local copies, waits for them, and re-layouts  24.3 us (3%)
  between operations  14.5 us (2%)
    all_gather x1, waiting for transfers between devices, body(): lax.all_gather(down_weight, 'sp', axis=1, tiled=True)  183 us
    all_gather x1, waiting for transfers between devices, body(): lax.all_gather(gate_weight, 'sp', axis=0, tiled=True)  141 us
    all_gather x1, waiting for transfers between devices, body(): lax.all_gather(up_weight, 'sp', axis=0, tiled=True)  135 us
    all_gather x2, waiting for transfers between devices, entering(): everything = jax.tree.map(lambda part: lax.all_gather(part, axis), value)  93 us
    select_n x48, other arithmetic, step(): return jax.tree.map(lambda a, b: jnp.where(reached, a, b), new, before)  55.7 us
    unnamed x1, blocking collectives  44.1 us
  transfers between devices with their start and end apart: 7, of which 6 were waited for; matrix products, arithmetic and copies ran while one was open for 6% of the time, Pallas kernels for 0%

commit v1 on v0

--- a/solution.py
+++ b/solution.py
@@ -193,7 +193,7 @@
     hidden = (jax.nn.silu(gate) * upper).astype(jnp.bfloat16)
     terms = jnp.dot(
         hidden,
-        lax.all_gather(down_weight, "sp", axis=1, tiled=True),
+        jnp.concatenate(lax.all_gather(down_weight, "sp"), axis=1),
         preferred_element_type=jnp.float32,
     )
     back = lax.psum_scatter(

time: 768 us -> 729 us (0.949)
  waiting for transfers between devices: 564 us -> 508 us
  local copies, waits for them, and re-layouts: 24.3 us -> 40.4 us
    all_gather x1, waiting for transfers between devices: 183 us -> 141 us  [body(): lax.all_gather(down_weight, 'sp')]
    reshape x0 -> x1, local copies, waits for them, and re-layouts: none -> 15.2 us  [body(): jnp.concatenate(lax.all_gather(down_weight, 'sp'), axis=1)]
    all_gather x1, waiting for transfers between devices: 141 us -> 127 us  [body(): lax.all_gather(gate_weight, 'sp', axis=0, tiled=True)]
  transfers between devices with their start and end apart: 7 -> 7, of which waited for: 6 -> 6; matrix products, arithmetic and copies ran while one was open for 6% -> 9% of each run, Pallas kernels for 0% -> 0%
where the time goes in v1:
time: 729 us; the launch traced here: 726 us
  waiting for transfers between devices  508 us (70%)
  other arithmetic  79.6 us (11%)
  blocking collectives  46.2 us (6%)
  local copies, waits for them, and re-layouts  40.4 us (6%)
  matrix products  36.9 us (5%)
  between operations  14.5 us (2%)
    all_gather x1, waiting for transfers between devices, body(): lax.all_gather(down_weight, 'sp')  141 us
    all_gather x1, waiting for transfers between devices, body(): lax.all_gather(up_weight, 'sp', axis=0, tiled=True)  135 us
    all_gather x1, waiting for transfers between devices, body(): lax.all_gather(gate_weight, 'sp', axis=0, tiled=True)  127 us
    all_gather x2, waiting for transfers between devices, entering(): everything = jax.tree.map(lambda part: lax.all_gather(part, axis), value)  92.5 us
    select_n x48, other arithmetic, step(): return jax.tree.map(lambda a, b: jnp.where(reached, a, b), new, before)  56.2 us
    unnamed x1, blocking collectives  43.8 us
    reshape x1, local copies, waits for them, and re-layouts, body(): jnp.concatenate(lax.all_gather(down_weight, 'sp'), axis=1)  15.2 us
  transfers between devices with their start and end apart: 7, of which 6 were waited for; matrix products, arithmetic and copies ran while one was open for 9% of the time, Pallas kernels for 0%

profile of v1, /device:TPU:0, one launch (start us, length us, event | category | flops | bytes accessed | tf_op | source)
XLA Modules:
  0.0 726.2 jit_solution(2016900786363241189)
XLA Ops:
  10.6 5.3 while.55
  20.6 19.5 %while.54 = (s32[]{:T(128)}, f32[4,128,256]{2,1,0:T(8,128)S(1)}, f32[4]{0:T(128)}, f32[2,64,4,256]{3,1,0,2:T(8,128)}, f32[2,4,64]{2,1,0:T(4,128)}, /*index=5*/f3...) while((s32[]{:T(128)}, f32[4,128,256]{2,1,0:T(8,128)S(1)}, ...), condition=%wide.region_4.5_spmd.clone, body=%wide.region_0.4_spmd.clone.sunk | while | flops 130980880 | bytes 3455009 | solution.py:75
  22.7 1.3 add_maximum_fusion.4
  26.6 1.1 fusion.152
  28.7 1.3 fusion.153
  32.7 1.3 add_maximum_fusion.4
  38.7 1.3 fusion.153
  41.0 1.6 copy.93
  42.6 1.2 dynamic-slice
  48.9 43.8 %all-reduce.4 = (f32[64]{0:T(128)S(1)}, f32[64]{0:T(128)S(1)}, f32[64]{0:T(128)S(1)}, f32[64]{0:T(128)S(1)}) all-reduce(f32[64]{0:T(128)S(1)} %dynamic-update-slice, f32[64]{0:T(128)S(1)} %dynamic-update-slice.1, f32[64]{0:T(128)S(1)} %dynamic-update-slice.2, f32[64]{0:T(128)S(1)} %dynamic-update-slice.3), channel_id=2, replica_groups=mesh['sp'=16,'tp'=2] {'sp'}, use_global_device_ids=true, to_apply=%add | all-reduce | flops 256 | bytes 2048
  97.0 1.1 copy.92
  98.1 1.2 copy.86
  99.3 1.3 convert_element_type.74
  100.6 1.2 convert_element_type.77
  101.8 92.5 %all-gather.17.cloned.1.call-done = f32[64,128,256]{2,1,0:T(8,128)} async-done(((f32[4,128,256]{2,1,0:T(8,128)}), f32[64,128,256]{2,1,0:T(8,128)}) %all-gather.17.cloned.1.call-update) | async-done | bytes 8388624 | tf_op jit(solution)/shard_map/all_gather | solution.py:13
  194.3 57.2 %while.56 = (s32[]{:T(128)}, f32[4,128,256]{2,1,0:T(8,128)S(1)}, f32[4]{0:T(128)}, f32[4,64,128]{2,1,0:T(8,128)S(1)}, f32[4]{0:T(128)}, /*index=5*/s32[]{:T(128)...) while((s32[]{:T(128)}, f32[4,128,256]{2,1,0:T(8,128)S(1)}, ...), condition=%wide.region_13.14_spmd.clone, body=%wide.region_12.13_spmd.clone.sunk | while | flops 819260 | bytes 1966609 | solution.py:25
  194.3 1.3 broadcast_select_fusion.9
  195.6 1.2 fusion.162
  197.9 1.3 broadcast_select_fusion.9
  199.2 1.2 fusion.162
  201.5 1.3 broadcast_select_fusion.9
  202.8 1.2 fusion.162
  205.1 1.3 broadcast_select_fusion.9
  206.4 1.2 fusion.162
  208.7 1.3 broadcast_select_fusion.9
  210.0 1.2 fusion.162
  212.2 1.3 broadcast_select_fusion.9
  213.6 1.2 fusion.162
  215.8 1.3 broadcast_select_fusion.9
  217.2 1.2 fusion.162
  219.4 1.3 broadcast_select_fusion.9
  220.8 1.2 fusion.162
  223.0 1.3 broadcast_select_fusion.9
  224.3 1.2 fusion.162
  226.6 1.3 broadcast_select_fusion.9
  227.9 1.2 fusion.162
  230.2 1.3 broadcast_select_fusion.9
  231.5 1.2 fusion.162
  233.7 1.3 broadcast_select_fusion.9
  235.0 1.2 fusion.162
  237.3 1.3 broadcast_select_fusion.9
  238.6 1.2 fusion.162
  240.9 1.3 broadcast_select_fusion.9
  242.2 1.2 fusion.162
  244.4 1.3 broadcast_select_fusion.9
  245.7 1.2 fusion.162
  248.0 1.3 broadcast_select_fusion.9
  249.3 1.2 fusion.162
  252.3 1.3 multiply_reduce_fusion.1
  254.3 1.1 copy.94
  255.4 1.5 multiply_reduce_fusion
  257.2 3.0 fusion.76
  260.3 1.3 fusion.67
  263.5 4.4 reduce-scatter.3.cloned.1.call-done
  267.9 1.1 fusion.72
  270.2 2.4 all_gather.55
  272.5 140.6 %all-gather.21.cloned.1.call-done = bf16[45056,128]{1,0:T(8,128)(2,1)} async-done(((bf16[2816,128]{1,0:T(8,128)(2,1)}), bf16[45056,128]{1,0:T(8,128)(2,1)}) %all-gather.21.cloned.1.call-update) | async-done | bytes 11534352 | tf_op jit(solution)/shard_map/all_gather | solution.py:196
  413.1 15.2 %copy.95 = bf16[2816,16,128]{0,2,1:T(8,128)(2,1)} copy(bf16[2816,16,128]{2,0,1:T(8,128)(2,1)} %bitcast.311) | data formatting | bytes 23068672 | tf_op jit(solution)/shard_map/reshape | solution.py:196
  428.3 127.0 %all-gather.13.cloned.1.call-done = bf16[2048,2816]{1,0:T(8,128)(2,1)} async-done(((bf16[128,2816]{1,0:T(8,128)(2,1)}), bf16[2048,2816]{1,0:T(8,128)(2,1)}) %all-gather.13.cloned.1.call-update) | async-done | bytes 11534352 | tf_op jit(solution)/shard_map/all_gather | solution.py:185
  555.3 7.1 fusion.118
  562.4 135.2 %all-gather.15.cloned.1.call-done = bf16[2048,2816]{1,0:T(8,128)(2,1)} async-done(((bf16[128,2816]{1,0:T(8,128)(2,1)}), bf16[2048,2816]{1,0:T(8,128)(2,1)}) %all-gather.15.cloned.1.call-update) | async-done | bytes 11534352 | tf_op jit(solution)/shard_map/all_gather | solution.py:190
  697.6 13.8 %convolution_convert_fusion = bf16[128,2048]{1,0:T(8,128)(2,1)} fusion(bf16[2816,2048]{0,1:T(8,128)(2,1)} %bitcast.312, bf16[128,2048]{1,0:T(8,128)(2,1)S(1)} %all_gather.55, bf16[2048,2816]{1,0:T(8,128)(2,1)} %all-gather.15.cloned.1.call-done, f32[128,2816]{1,0:T(8,128)} %fusion.118), kind=kOutput, calls=%fused_computation.130 | convolution fusion | flops 2955214848 | bytes 25559040 | tf_op jit(solution)/shard_map/dot_general | solution.py:194
  711.4 6.3 reduce-scatter.5.cloned.1.call-done
  717.6 1.7 fusion.75
  (223 shorter events, 57.7 us)
Async XLA Ops:
  6.5 253.8 %copy-start = (bf16[512,2048]{1,0:T(8,128)(2,1)S(1)}, bf16[512,2048]{1,0:T(8,128)(2,1)}, u32[]{:S(2)}) copy-start(bf16[512,2048]{1,0:T(8,128)(2,1)} %param.39) | copy-start | bytes 6291460
  6.5 95.3 %all-gather.19.cloned.1.call-start = ((), (), s32[]{:S(2)}) async-start(), calls=%async_computation.7 | async-start | bytes 2228224 | tf_op jit(solution)/shard_map/all_gather | solution.py:13
  10.6 6.1 copy-start.14
  10.6 6.9 copy-start.8
  10.6 8.1 %copy-start.7 = (bf16[128,512]{1,0:T(8,128)(2,1)S(1)}, bf16[128,512]{1,0:T(8,128)(2,1)}, u32[]{:S(2)}) copy-start(bf16[128,512]{1,0:T(8,128)(2,1)} %param.26) | copy-start | bytes 393220
  15.9 0.6 copy-start.3
  15.9 4.6 copy-start.11
  15.9 4.6 copy-start.15
  16.6 177.7 %all-gather.17.cloned.1.call-start = ((), (), s32[]{:S(2)}) async-start(), calls=%async_computation.6 | async-start | bytes 8912896 | tf_op jit(solution)/shard_map/all_gather | solution.py:13
  21.3 2.7 copy-start.6
  21.9 2.0 copy-start.9
  30.7 3.3 copy-start.6
  32.0 2.0 copy-start.9
  40.1 0.8 copy-start.2
  40.9 227.0 %reduce-scatter.3.cloned.1.call-start = ((), (), s32[]{:S(2)}) async-start(), calls=%async_computation.2 | async-start | bytes 786432 | tf_op jit(solution)/shard_map/reduce_scatter | solution.py:171
  47.0 51.0 %copy-start.12 = (f32[4,128]{1,0:T(4,128)}, f32[4,128]{1,0:T(4,128)S(1)}, u32[]{:S(2)}) copy-start(f32[4,128]{1,0:T(4,128)S(1)} %reduce_window_sum.38) | copy-start | bytes 6148
  48.5 49.6 %copy-start.13 = (f32[4,128]{1,0:T(4,128)}, f32[4,128]{1,0:T(4,128)S(1)}, u32[]{:S(2)}) copy-start(f32[4,128]{1,0:T(4,128)S(1)} %reduce_window_sum.39) | copy-start | bytes 6148
  251.5 5.7 copy-start.18
  256.9 3.4 copy-start.10
  257.0 3.4 copy-start.16
  260.3 3.1 copy-start.17
  260.3 7.6 %copy-start.4 = (bf16[64,2048]{1,0:T(8,128)(2,1)S(1)}, bf16[64,2048]{1,0:T(8,128)(2,1)}, u32[]{:S(2)}) copy-start(bf16[64,2048]{1,0:T(8,128)(2,1)} %param.25) | copy-start | bytes 786436
  261.7 151.4 %all-gather.21.cloned.1.call-start = ((), (), s32[]{:S(2)}) async-start(), calls=%async_computation.8 | async-start | bytes 12255232 | tf_op jit(solution)/shard_map/all_gather | solution.py:196
  262.2 293.1 %all-gather.13.cloned.1.call-start = ((), (), s32[]{:S(2)}) async-start(), calls=%async_computation.3 | async-start | bytes 12255232 | tf_op jit(solution)/shard_map/all_gather | solution.py:185
  262.8 434.7 %all-gather.15.cloned.1.call-start = ((), (), s32[]{:S(2)}) async-start(), calls=%async_computation.4 | async-start | bytes 12255232 | tf_op jit(solution)/shard_map/all_gather | solution.py:190
  263.4 454.2 %reduce-scatter.5.cloned.1.call-start = ((), (), s32[]{:S(2)}) async-start(), calls=%async_computation.5 | async-start | bytes 786432 | tf_op jit(solution)/shard_map/reduce_scatter | solution.py:199
  697.6 20.1 %copy-start.5 = (bf16[64,2048]{1,0:T(8,128)(2,1)S(1)}, bf16[64,2048]{1,0:T(8,128)(2,1)}, u32[]{:S(2)}) copy-start(bf16[64,2048]{1,0:T(8,128)(2,1)} %reduce-scatter.3.cloned.1.call-done) | copy-start | bytes 786436
  697.6 21.8 %copy-start.1 = (bf16[512,2048]{1,0:T(8,128)(2,1)S(1)}, bf16[512,2048]{1,0:T(8,128)(2,1)}, u32[]{:S(2)}) copy-start(bf16[512,2048]{1,0:T(8,128)(2,1)} %param.39) | copy-start | bytes 6291460
Sparse Core Ops, SparseCore 0:
  16.7 63.6 all-gather.18
  83.2 111.0 all-gather.16
  261.8 6.0 reduce-scatter.2
  270.5 142.5 all-gather.20
  415.7 139.5 all-gather.12
  557.9 139.5 all-gather.14
  711.5 6.0 reduce-scatter.4
